TPU v7x, 32 devices: a whole 2x2x4 slice. The times are simulated.
32 devices in a mesh: grp: 2 (over y), fs: 4 (over z), tp: 4 (over x, core).
Axes of the slice: x: 2, y: 2, z: 4, core: 2. Of those that a mesh axis runs over, the one named last changes fastest.
Arguments:
- stream: bfloat16 [2048, 3072], P('tp', ('grp', 'fs')), parts along dimension 1, may hold values from -6 to 6
- first_gain: float32 [2048], replicated, may hold values from 0.1 to 1.9
- first_gate: float32 [2048, 5632], P('fs', 'tp'), may hold values from -0.125 to 0.125
- first_gate_scale: float32 [5632], P('tp'), may hold values from 0.5 to 2
- first_up: float32 [2048, 5632], P('fs', 'tp'), may hold values from -0.125 to 0.125
- first_up_scale: float32 [5632], P('tp'), may hold values from 0.5 to 2
- first_down: float32 [5632, 2048], P('tp', 'fs'), may hold values from -0.078125 to 0.078125
- first_down_scale: float32 [2048], P('fs'), may hold values from 0.5 to 2
- mixer_gain: float32 [2048], replicated, may hold values from 0.1 to 1.9
- mixer_left: float32 [2048, 1024], P('fs', 'tp'), may hold values from -0.125 to 0.125
- mixer_left_scale: float32 [1024], P('tp'), may hold values from 0.5 to 2
- mixer_right: float32 [2048, 1024], P('fs', 'tp'), may hold values from -0.125 to 0.125
- mixer_right_scale: float32 [1024], P('tp'), may hold values from 0.5 to 2
- channel_gain: float32 [1024], P('tp'), may hold values from 0.1 to 1.9
- spatial: bfloat16 [8, 128, 128], P('tp'), may hold values from -0.5 to 0.5
- spatial_bias: float32 [8, 128], P('tp'), may hold values from 0.1 to 1.9
- mixer_out: float32 [1024, 2048], P('tp', 'fs'), may hold values from -0.1875 to 0.1875
- mixer_out_scale: float32 [2048], P('fs'), may hold values from 0.5 to 2
- second_gain: float32 [2048], replicated, may hold values from 0.1 to 1.9
- second_gate: float32 [2048, 5632], P('fs', 'tp'), may hold values from -0.125 to 0.125
- second_gate_scale: float32 [5632], P('tp'), may hold values from 0.5 to 2
- second_up: float32 [2048, 5632], P('fs', 'tp'), may hold values from -0.125 to 0.125
- second_up_scale: float32 [5632], P('tp'), may hold values from 0.5 to 2
- second_down: float32 [5632, 2048], P('tp', 'fs'), may hold values from -0.078125 to 0.078125
- second_down_scale: float32 [2048], P('fs'), may hold values from 0.5 to 2
Outputs:
- result: bfloat16 [2048, 3072], P('tp', ('grp', 'fs')), parts along dimension 1
There are 2 independent parts, one for each index of `grp`. A program takes and returns all parts, laid end to end along the dimension named above; an argument that names none is the same for every part. Nothing has to cross between parts.
All inputs are finite; a program needn't handle non-finite values.
Results may differ from a plain program's by a relative error of at most 0.02.
Values may be sent and summed in bfloat16 or wider, within the bound.
A program may use at most 128 MiB of HBM per device.

v0:
```python
import jax
import jax.numpy as jnp
from jax import lax
from jax.experimental import pallas as pl
from jax.experimental.pallas import tpu as pltpu
from jax.sharding import PartitionSpec as P

EPS = 1e-06
CORES = 2
LANES = 128
CHUNKS = 2
MESH = pl.DeviceIdType.MESH
F32, BF16 = jnp.float32, jnp.bfloat16


def many(count):
    return pltpu.SemaphoreType.DMA((count,))


def kernel(
    stream, gate_1, up_1, down_1, left_w, right_w, out_w, gate_2, up_2, down_2,
    gain_1, gain_m, gain_2, gate_scale_1, up_scale_1, down_scale_1, left_scale, right_scale, out_scale,
    gate_scale_2, up_scale_2, down_scale_2, channel_gain, spatial, spatial_bias,
    result,
    weights, mixer_w, staged, turned, wide_in, tall_in, mixer_in,
    rows_1, rows_m, rows_2, normal, hidden, gated, held, kept, stats,
    core_out, core_out_m, core_in_1, core_in_m, core_in_2,
    chip_out, chip_out_m, chip_in_1, chip_in_m, chip_in_2,
    pair_out, pair_in_1, pair_in_2,
    send_sem, recv_sem, load_sem,
):
    grp, fs, tp = lax.axis_index("grp"), lax.axis_index("fs"), lax.axis_index("tp")
    groups, count, tps = lax.axis_size("grp"), lax.axis_size("fs"), lax.axis_size("tp")
    half = count // 2
    side = fs // half
    partner = lax.rem(fs + half, count)
    near = side * half + (1 - lax.rem(fs, half))
    core, chip = lax.rem(tp, CORES), tp // CORES
    sibling = chip * CORES + (1 - core)
    across = lax.rem(tp + CORES, tps)
    diagonal = lax.rem(sibling + CORES, tps)
    wide, tokens = stream.shape
    share = wide // groups
    tall = hidden.shape[1]
    part = tokens // CHUNKS
    branch = left_w.shape[1]

    to_partner, to_near = {"fs": partner}, {"fs": near}
    to_group = {"grp": 1 - grp}
    to_sibling, to_across, to_diagonal = {"tp": sibling}, {"tp": across}, {"tp": diagonal}
    every = (to_partner, to_near, to_group, to_sibling, to_across, to_diagonal)

    barrier = pltpu.get_barrier_semaphore()
    for device in every:
        pl.semaphore_signal(barrier, inc=1, device_id=device, device_id_type=MESH)

    used = [0, 0]
    pending = []

    def send(source, target, device):
        at = used[0]
        used[0] += 1
        copy = pltpu.make_async_remote_copy(
            src_ref=source,
            dst_ref=target,
            send_sem=send_sem.at[at],
            recv_sem=recv_sem.at[at],
            device_id=device,
            device_id_type=MESH,
        )
        copy.start()
        pending.append(copy)
        return copy

    def sent(copies):
        for copy in copies:
            copy.wait_send()
        pending[:] = [other for other in pending if all(other is not copy for copy in copies)]

    def load(source, target):
        at = used[1]
        used[1] += 1
        copy = pltpu.make_async_copy(source, target, load_sem.at[at])
        copy.start()
        return copy

    def place(source, member):
        return pl.ds(pl.multiple_of((source * groups + member) * share, share), share)

    def of_share(member):
        return pl.ds(pl.multiple_of(member * share, share), share)

    own_side = pl.ds(pl.multiple_of(side * tall, 16), tall)
    other_side = pl.ds(pl.multiple_of((1 - side) * tall, 16), tall)


    def load_rows(weight, member, slot):
        return load(weight.at[of_share(member), :], wide_in.at[slot])

    def load_cols(weight, member):
        return load(weight.at[:, of_share(member)], tall_in)

    def load_mixer(member, slot):
        return [
            load(left_w.at[of_share(member), :], mixer_in.at[slot, 0]),
            load(right_w.at[of_share(member), :], mixer_in.at[slot, 1]),
            load(out_w.at[:, of_share(member)], mixer_in.at[slot, 2]),
        ]

    def turn(slot, scale, target):
        def step(at, carry):
            lanes = pl.ds(pl.multiple_of(at * LANES, LANES), LANES)
            target[lanes, :] = (wide_in[slot, :, lanes] * scale[:, lanes]).T.astype(BF16)
            return carry

        lax.fori_loop(0, wide_in.shape[2] // LANES, step, 0)

    def cast_rows(unit, stage, slot, scale):
        target = turned if stage is None else staged.at[stage]
        turn(slot, scale, target)
        member = 1 - grp if stage is None else grp
        weights[unit, :, place(fs, member)] = target[own_side, :]

    def cast_cols(unit, stage, scale):
        member = 1 - grp if stage is None else grp
        factor = scale[:, of_share(member)]
        weights[unit, :, place(fs, member)] = (tall_in[own_side, :] * factor).astype(BF16)
        if stage is not None:
            staged[stage, 0:tall, :] = (tall_in[other_side, :] * factor).astype(BF16)

    def cast_mixer(slot, member):
        at = fs * groups + member
        mixer_w[at, 0:share, :] = (mixer_in[slot, 0] * left_scale[...]).astype(BF16)
        mixer_w[at, share : 2 * share, :] = (mixer_in[slot, 1] * right_scale[...]).astype(BF16)
        mixer_w[at, 2 * share : 3 * share, :] = (
            mixer_in[slot, 2] * out_scale[:, of_share(member)]
        ).astype(BF16)

    class Unit:
        def __init__(self, slot, source):
            self.slot, self.source = slot, source

        def begin(self):
            mine = self.slot(fs, grp)
            self.first = send(self.source() if self.source else mine, mine, to_partner)
            self.second = send(mine, mine, to_near)

        def relay_first(self):
            self.first.wait_recv()
            got = self.slot(partner, grp)
            self.third = send(got, got, to_near)
            self.swaps = [send(got, got, to_group)]

        def relay_second(self):
            self.second.wait_recv()
            got = self.slot(near, grp)
            self.swaps.append(send(got, got, to_group))

        def relay_third(self):
            self.third.wait_recv()
            got = self.slot(lax.rem(near + half, count), grp)
            self.swaps.append(send(got, got, to_group))

        def complete(self):
            for copy in self.swaps:
                copy.wait_recv()

    def hidden_unit(unit, stage, turns):
        return Unit(
            lambda source, member: weights.at[unit, :, place(source, member)],
            lambda: staged.at[stage, other_side if turns else pl.ds(0, tall), :],
        )

    g1, u1, d1 = hidden_unit(0, 0, True), hidden_unit(1, 1, True), hidden_unit(2, 2, False)
    g2, u2, d2 = hidden_unit(3, 0, True), hidden_unit(4, 1, True), hidden_unit(5, 2, False)
    mixer = Unit(lambda source, member: mixer_w.at[source * groups + member], None)


    def gather_begin(rows, pair):
        def view(at_side, at_tp, at):
            first = at_side * tokens + at * part if pair else at * part
            return rows.at[
                pl.ds(pl.multiple_of(first, part), part),
                pl.ds(pl.multiple_of(at_tp * wide, wide), wide),
            ]

        firsts, chips, cores = [], [], []
        for at in range(CHUNKS):
            mine = view(side, tp, at)
            if pair:
                firsts.append(send(mine, mine, to_partner))
            chips.append(send(mine, mine, to_across))
            cores.append(send(mine, mine, to_sibling))
        return view, firsts, chips, cores

    def gather_end(begun):
        view, firsts, chips, cores = begun
        seconds = []
        for at in range(CHUNKS):
            if firsts:
                firsts[at].wait_recv()
                got = view(1 - side, tp, at)
                seconds.append(send(got, got, to_across))
                cores.append(send(got, got, to_sibling))
            chips[at].wait_recv()
            got = view(side, across, at)
            cores.append(send(got, got, to_sibling))
        for at, copy in enumerate(seconds):
            copy.wait_recv()
            got = view(1 - side, across, at)
            cores.append(send(got, got, to_sibling))
        for copy in cores:
            copy.wait_recv()

    def own_rows(rows, pair):
        first = pl.multiple_of(side * tokens, part) if pair else 0
        rows[pl.ds(first, tokens), pl.ds(pl.multiple_of(tp * wide, wide), wide)] = held[...]

    def norm(rows, gain):
        size = 64

        def step(at, carry):
            here = pl.ds(pl.multiple_of(at * size, size), size)
            values = rows[here, :].astype(F32)
            inverse = lax.rsqrt(jnp.mean(values * values, axis=1, keepdims=True) + EPS)
            normal[here, :] = (values * inverse * gain[...]).astype(BF16)
            return carry

        lax.fori_loop(0, rows.shape[0] // size, step, 0)

    def expand(unit):
        def step(at, carry):
            here = pl.ds(pl.multiple_of(at * tokens, tokens), tokens)
            values = normal[here, :]
            dims = (((1,), (1,)), ((), ()))
            gate = lax.dot_general(values, weights[unit], dims, preferred_element_type=F32)
            upward = lax.dot_general(values, weights[unit + 1], dims, preferred_element_type=F32)
            hidden[here, :] = (gate / (1.0 + jnp.exp(-gate)) * upward).astype(BF16)
            return carry

        lax.fori_loop(0, 2, step, 0)

    def reduce_sums(tiles, product, outs, ins, between):
        core_to, chip_to, pair_to = outs
        core_from, chip_from, pair_from = ins
        firsts, seconds, thirds = {}, {}, {}

        def begin(at):
            for to_chip in range(tps // CORES):
                other = to_chip * CORES + 1 - core
                core_to[at, to_chip] = product(tiles[at][0], other).astype(BF16)
            firsts[at] = send(core_to.at[at], core_from.at[at], to_sibling)
            for to_chip in range(tps // CORES):
                kept[at, to_chip] = product(tiles[at][0], to_chip * CORES + core)

        def chips(at):
            firsts[at].wait_recv()
            away = 1 - chip
            chip_to[at] = (kept[at, away] + core_from[at, away].astype(F32)).astype(BF16)
            seconds[at] = send(chip_to.at[at], chip_from.at[at], to_across)
            kept[at, chip] = kept[at, chip] + core_from[at, chip].astype(F32)

        def pairs(at):
            seconds[at].wait_recv()
            total = kept[at, chip] + chip_from[at].astype(F32)
            if tiles[at][1]:
                pair_to[at] = total.astype(BF16)
                thirds[at] = send(pair_to.at[at], pair_from.at[at], to_partner)
            else:
                kept[at, chip] = total

        for at in range(len(tiles) + 2):
            if at < len(tiles):
                begin(at)
            if 0 <= at - 1 < len(tiles):
                chips(at - 1)
            if 0 <= at - 2 < len(tiles):
                pairs(at - 2)
            between(at)
        own = [at for at in range(len(tiles)) if not tiles[at][1]]
        for order, at in enumerate(own):
            total = kept[at, chip]
            if thirds:
                thirds[order].wait_recv()
                total = total + pair_from[order].astype(F32)
            here = pl.ds(order * part, part)
            factor = 0.5 if thirds else 1.0
            held[here, :] = (held[here, :].astype(F32) + factor * total).astype(BF16)
        return list(firsts.values()) + list(seconds.values()) + list(thirds.values())

    def half_tiles():
        away = [((1 - side) * tokens + at * part, True) for at in range(CHUNKS)]
        return away + [(side * tokens + at * part, False) for at in range(CHUNKS)]

    def down_product(unit):
        def product(first, target):
            values = hidden[pl.ds(pl.multiple_of(first, part), part), :]
            columns = pl.ds(pl.multiple_of(target * wide, wide), wide)
            return jnp.dot(values, weights[unit, :, columns], preferred_element_type=F32)

        return product


    def nothing(at):
        pass

    loads = {"g1": load_rows(gate_1, grp, 0), "u1": load_rows(up_1, grp, 1), "d1": load_cols(down_1, grp)}
    held[...] = stream[...].astype(F32).T.astype(BF16)
    own_rows(rows_1, True)
    pl.semaphore_wait(barrier, len(every))
    begun = gather_begin(rows_1, True)

    loads["g1"].wait()
    cast_rows(0, 0, 0, gate_scale_1)
    g1.begin()
    loads["g1"] = load_rows(gate_1, 1 - grp, 0)
    loads["u1"].wait()
    cast_rows(1, 1, 1, up_scale_1)
    u1.begin()
    loads["u1"] = load_rows(up_1, 1 - grp, 1)
    loads["d1"].wait()
    cast_cols(2, 2, down_scale_1)
    d1.begin()
    loads["d1"] = load_cols(down_1, 1 - grp)
    loads["m"] = load_mixer(grp, 0)
    loads["n"] = load_mixer(1 - grp, 1)
    gather_end(begun)
    g1.relay_first()
    g1.relay_second()
    loads["g1"].wait()
    cast_rows(0, None, 0, gate_scale_1)
    loads["g2"] = load_rows(gate_2, grp, 0)
    u1.relay_first()
    u1.relay_second()
    loads["u1"].wait()
    cast_rows(1, None, 1, up_scale_1)
    loads["u2"] = load_rows(up_2, grp, 1)
    d1.relay_first()
    d1.relay_second()
    loads["d1"].wait()
    cast_cols(2, None, down_scale_1)
    loads["d2"] = load_cols(down_2, grp)
    norm(rows_1, gain_1)
    for copy in loads["m"] + loads["n"]:
        copy.wait()
    cast_mixer(0, grp)
    cast_mixer(1, 1 - grp)
    g1.relay_third()
    sent([g1.first, u1.first, d1.first])
    loads["g2"].wait()
    cast_rows(3, 0, 0, gate_scale_2)
    loads["g2"] = load_rows(gate_2, 1 - grp, 0)
    u1.relay_third()
    loads["u2"].wait()
    cast_rows(4, 1, 1, up_scale_2)
    loads["u2"] = load_rows(up_2, 1 - grp, 1)
    d1.relay_third()
    mixer.begin()
    g1.complete()
    u1.complete()
    expand(0)
    d1.complete()

    def between_1(at):
        if at == 4:
            mixer.relay_first()
            mixer.relay_second()

    copies = reduce_sums(
        half_tiles(), down_product(2), (core_out, chip_out, pair_out),
        (core_in_1, chip_in_1, pair_in_1), between_1,
    )

    own_rows(rows_m, False)
    begun = gather_begin(rows_m, False)
    g2.begin()
    u2.begin()
    mixer.relay_third()
    loads["d2"].wait()
    cast_cols(5, 2, down_scale_2)
    loads["d2"] = load_cols(down_2, 1 - grp)
    gather_end(begun)
    norm(rows_m, gain_m)
    mixer.complete()

    def projection(first):
        total = None
        for at in range(count * groups):
            term = jnp.dot(
                normal[0:tokens, at * share : (at + 1) * share],
                mixer_w[at, first : first + share, :],
                preferred_element_type=F32,
            )
            total = term if total is None else total + term
        return jax.nn.gelu(total)

    right = projection(share)
    lane = lax.broadcasted_iota(jnp.int32, (tokens, LANES), 1)
    sums = jnp.sum(right, axis=1, keepdims=True)
    squares = jnp.sum(right * right, axis=1, keepdims=True)
    packed = jnp.where(lane == 0, sums, jnp.where(lane == 1, squares, 0.0))
    stats[0] = packed.T[0:8, :]
    shared = [
        send(stats.at[0], stats.at[1], to_sibling),
        send(stats.at[0], stats.at[2], to_across),
        send(stats.at[0], stats.at[3], to_diagonal),
    ]
    left = projection(0)
    for copy in shared:
        copy.wait_recv()
    total = (stats[0] + stats[1]) + (stats[2] + stats[3])
    total = jnp.concatenate([total, jnp.zeros((LANES - 8, tokens), F32)], axis=0).T
    size = branch * tps
    average = total[:, 0:1] / size
    inverse = lax.rsqrt(total[:, 1:2] / size - average * average + EPS)
    centred = ((right - average) * inverse * channel_gain[...]).astype(BF16)
    span = spatial.shape[1]
    target = lax.broadcasted_iota(jnp.int32, (span, span), 0)
    source = lax.broadcasted_iota(jnp.int32, (span, span), 1)
    members = branch // spatial.shape[0]
    for group in range(spatial.shape[0]):
        matrix = jnp.where(source <= target, spatial[group].astype(F32), 0.0).astype(BF16)
        columns = slice(group * members, (group + 1) * members)
        for at in range(tokens // span):
            here = slice(at * span, (at + 1) * span)
            mixed = jnp.dot(matrix, centred[here, columns], preferred_element_type=F32)
            mixed = mixed + spatial_bias[:, group : group + 1]
            gated[here, columns] = (left[here, columns] * mixed).astype(BF16)
    g2.relay_first()
    g2.relay_second()

    def out_product(first, target):
        values = gated[first : first + part, :]
        each = wide // share
        return jnp.concatenate(
            [
                jnp.dot(
                    values,
                    mixer_w[target * each + at, 2 * share : 3 * share, :],
                    preferred_element_type=F32,
                )
                for at in range(each)
            ],
            axis=1,
        )

    reduce_sums(
        [(at * part, False) for at in range(CHUNKS)], out_product, (core_out_m, chip_out_m, None),
        (core_in_m, chip_in_m, None), nothing,
    )

    own_rows(rows_2, True)
    begun = gather_begin(rows_2, True)
    d2.begin()
    u2.relay_first()
    u2.relay_second()
    g2.relay_third()
    loads["g2"].wait()
    cast_rows(3, None, 0, gate_scale_2)
    loads["u2"].wait()
    cast_rows(4, None, 1, up_scale_2)
    loads["d2"].wait()
    cast_cols(5, None, down_scale_2)
    gather_end(begun)
    norm(rows_2, gain_2)
    u2.relay_third()
    d2.relay_first()
    d2.relay_second()
    g2.complete()
    u2.complete()
    expand(3)
    d2.relay_third()
    d2.complete()
    sent(copies)
    reduce_sums(
        half_tiles(), down_product(5), (core_out, chip_out, pair_out),
        (core_in_2, chip_in_2, pair_in_2), nothing,
    )
    result[...] = held[...].astype(F32).T.astype(BF16)
    for copy in list(pending):
        copy.wait_send()


def contract(left_side, right_side):
    return lax.dot_general(
        left_side, right_side, (((0,), (0,)), ((), ())), preferred_element_type=jnp.float32
    )


def product(left_side, right_side):
    return lax.dot_general(
        left_side, right_side, (((1,), (0,)), ((), ())), preferred_element_type=jnp.float32
    )


def permuted(block, axis_name, target):
    count = lax.axis_size(axis_name)
    return lax.ppermute(block, axis_name, [(at, target(at, count)) for at in range(count)])


def to_partner(block):
    return permuted(block, "fs", lambda at, count: (at + count // 2) % count)


def in_half(block, step):
    def target(at, count):
        half = count // 2
        return at // half * half + (at % half + step) % half

    return permuted(block, "fs", target)


def to_other_grp(block, step):
    return permuted(block, "grp", lambda at, count: (at + step) % count)


def to_same_core(block, step):
    return permuted(block, "tp", lambda at, count: (at + step * CORES) % count)


def to_other_core(block):
    return permuted(block, "tp", lambda at, count: at ^ 1)


def pick(blocks, index):
    count = len(blocks)
    if count == 1:
        return blocks[0]
    index = lax.rem(index + count, count)
    found = blocks[0]
    for at in range(1, count):
        found = jnp.where(index == at, blocks[at], found)
    return found


def chip_and_core():
    place = lax.axis_index("tp")
    return lax.div(place, CORES), lax.rem(place, CORES)


def gather_rows(block):
    chips = lax.axis_size("tp") // CORES
    chip, core = chip_and_core()
    held = jnp.stack([block] + [to_same_core(block, step) for step in range(1, chips)])
    other = to_other_core(held)
    found = []
    for at_chip in range(chips):
        mine = pick([held[step] for step in range(chips)], chip - at_chip)
        theirs = pick([other[step] for step in range(chips)], chip - at_chip)
        found += [jnp.where(core == 0, mine, theirs), jnp.where(core == 0, theirs, mine)]
    return jnp.concatenate(found)


def scatter_sum(terms):
    chips = lax.axis_size("tp") // CORES
    chip, core = chip_and_core()
    blocks = terms.reshape((chips, CORES, -1) + terms.shape[1:])
    mine = jnp.where(core == 0, blocks[:, 0], blocks[:, 1])
    passed = jnp.where(core == 0, blocks[:, 1], blocks[:, 0])
    pairs = mine.astype(jnp.float32) + to_other_core(passed).astype(jnp.float32)
    total = pick([pairs[at] for at in range(chips)], chip)
    for step in range(1, chips):
        sent = pick([pairs[at] for at in range(chips)], chip + step).astype(jnp.bfloat16)
        total = total + to_same_core(sent, step).astype(jnp.float32)
    return total


def places():
    count = lax.axis_size("fs")
    half = count // 2
    me = lax.axis_index("fs")
    low = lax.rem(me, half)
    found = []
    for step in range(half):
        near = me - low + lax.rem(low - step + half, half)
        found += [near, lax.rem(near + half, count)]
    return found


def shares():
    count = lax.axis_size("grp")
    me = lax.axis_index("grp")
    return [lax.rem(me - back + count, count) for back in range(count)]


def gathered(kept, passed, others):
    half = lax.axis_size("fs") // 2
    got = to_partner(passed)
    mine = [kept, got]
    for step in range(1, half):
        mine += [in_half(kept, step), in_half(got, step)]
    found = [mine]
    for back, own in zip(range(1, lax.axis_size("grp")), others):
        found.append([own] + [to_other_grp(block, back) for block in mine[1:]])
    return found


def rows_unit(weights):
    half = lax.div(lax.axis_index("fs"), lax.axis_size("fs") // 2)

    def cut(index, side):
        found = []
        for weight in weights:
            width = weight.shape[0] // lax.axis_size("grp")
            wide = weight.shape[1] // 2
            part = lax.dynamic_slice(weight, (index * width, side * wide), (width, wide))
            found.append(part.astype(jnp.bfloat16).T)
        return jnp.stack(found)

    order = shares()
    return gathered(
        cut(order[0], half), cut(order[0], 1 - half), [cut(index, half) for index in order[1:]]
    )


def cols_unit(weight):
    half = lax.div(lax.axis_index("fs"), lax.axis_size("fs") // 2)

    def cut(index, side):
        width = weight.shape[1] // lax.axis_size("grp")
        tall = weight.shape[0] // 2
        part = lax.dynamic_slice(weight, (side * tall, index * width), (tall, width))
        return part.astype(jnp.bfloat16)

    order = shares()
    return gathered(
        cut(order[0], half), cut(order[0], 1 - half), [cut(index, half) for index in order[1:]]
    )


def mixer_unit(left, right, out):
    def cut(index):
        width = left.shape[0] // lax.axis_size("grp")
        rows = [
            lax.dynamic_slice_in_dim(weight, index * width, width, 0).astype(jnp.bfloat16).T
            for weight in (left, right)
        ]
        return jnp.stack(rows + [lax.dynamic_slice_in_dim(out, index * width, width, 1).astype(jnp.bfloat16)])

    order = shares()
    share = cut(order[0])
    return gathered(share, share, [cut(index) for index in order[1:]])


def rows_in_order(rows):
    count, groups = lax.axis_size("fs"), lax.axis_size("grp")
    width = rows.shape[0] // (count * groups)
    pieces = []
    for share in shares():
        for place in places():
            pieces.append(
                lax.dynamic_slice_in_dim(rows, (place * groups + share) * width, width, 0)
            )
    return jnp.concatenate(pieces)


def joined(blocks):
    return jnp.concatenate([block for mine in blocks for block in mine], axis=-1)


def columns_out(blocks, hidden):
    count, groups = lax.axis_size("fs"), lax.axis_size("grp")
    every = joined(blocks)
    width = every.shape[1] // (count * groups)
    terms = contract(every, hidden).astype(jnp.bfloat16)
    found = jnp.zeros_like(terms)
    at = 0
    for share in shares():
        for place in places():
            found = lax.dynamic_update_slice_in_dim(
                found, terms[at : at + width], (place * groups + share) * width, 0
            )
            at += width
    return found


def inverse_of(values):
    return lax.rsqrt(jnp.mean(values * values, axis=0) + EPS)


def normed(whole_rows, gain):
    values = whole_rows.astype(jnp.float32)
    return (values * inverse_of(values) * gain[:, None]).astype(jnp.bfloat16)


def half_step(stream, gain, rows_blocks, gate_scale, up_scale, cols_blocks, down_scale):
    tokens = stream.shape[1]
    both = jnp.concatenate([stream, to_partner(stream)], axis=1)
    rows = rows_in_order(normed(gather_rows(both), gain))
    half = lax.div(lax.axis_index("fs"), lax.axis_size("fs") // 2)
    tall = gate_scale.shape[0] // 2
    gate_scale = lax.dynamic_slice_in_dim(gate_scale, half * tall, tall)[:, None]
    up_scale = lax.dynamic_slice_in_dim(up_scale, half * tall, tall)[:, None]
    every = joined(rows_blocks)
    gate = product(every[0], rows)
    upward = product(every[1], rows)
    hidden = (jax.nn.silu(gate * gate_scale) * (upward * up_scale)).astype(jnp.bfloat16)
    total = scatter_sum(columns_out(cols_blocks, hidden))
    away = to_partner(total[:, tokens:].astype(jnp.bfloat16))
    total = total[:, :tokens] + away.astype(jnp.float32)
    return (stream.astype(jnp.float32) + 0.5 * (total * down_scale[:, None])).astype(jnp.bfloat16)


def gating_unit(left_pre, right_pre, channel_gain, spatial, spatial_bias):
    left = jax.nn.gelu(left_pre)
    right = jax.nn.gelu(right_pre)
    branch = channel_gain.shape[0] * lax.axis_size("tp")
    totals, squares = lax.psum((jnp.sum(right, axis=0), jnp.sum(right * right, axis=0)), "tp")
    average = totals / branch
    inverse = lax.rsqrt(squares / branch - average * average + EPS)
    centred = ((right - average) * inverse * channel_gain[:, None]).astype(jnp.bfloat16)
    local_groups, span = (spatial.shape[0], spatial.shape[1])
    tokens = centred.shape[1]
    blocks = centred.reshape(local_groups, centred.shape[0] // local_groups, tokens // span, span)
    target = lax.broadcasted_iota(jnp.int32, (span, span), 0)
    source = lax.broadcasted_iota(jnp.int32, (span, span), 1)
    masked = jnp.where((source <= target)[None], spatial, jnp.zeros_like(spatial))
    token_mix = jnp.einsum("gts,gcns->gcnt", masked, blocks, preferred_element_type=jnp.float32)
    token_mix = token_mix + spatial_bias[:, None, None, :]
    return (left * token_mix.reshape(centred.shape[0], tokens)).astype(jnp.bfloat16)


def layer(
    stream,
    first_gain,
    first_gate,
    first_gate_scale,
    first_up,
    first_up_scale,
    first_down,
    first_down_scale,
    mixer_gain,
    mixer_left,
    mixer_left_scale,
    mixer_right,
    mixer_right_scale,
    channel_gain,
    spatial,
    spatial_bias,
    mixer_out,
    mixer_out_scale,
    second_gain,
    second_gate,
    second_gate_scale,
    second_up,
    second_up_scale,
    second_down,
    second_down_scale,
):
    held = jnp.stack([first_down_scale, mixer_out_scale, second_down_scale])
    count = lax.axis_size("fs")
    me = lax.axis_index("fs")
    parts = [held] + [
        permuted(held, "fs", lambda at, count, step=step: (at + step) % count)
        for step in range(1, count)
    ]
    scales = jnp.concatenate([pick(parts, me - place) for place in range(count)], axis=1)
    wide = stream.shape[0]
    scales = lax.dynamic_slice_in_dim(scales, lax.axis_index("tp") * wide, wide, 1)

    first_rows = rows_unit((first_gate, first_up))
    first_cols = cols_unit(first_down)
    mixer = mixer_unit(mixer_left, mixer_right, mixer_out)
    second_rows = rows_unit((second_gate, second_up))
    second_cols = cols_unit(second_down)

    stream = half_step(
        stream, first_gain, first_rows, first_gate_scale, first_up_scale, first_cols, scales[0]
    )
    rows = rows_in_order(normed(gather_rows(stream), mixer_gain))
    lefts = joined([[block[0] for block in mine] for mine in mixer])
    rights = joined([[block[1] for block in mine] for mine in mixer])
    gated = gating_unit(
        product(lefts, rows) * mixer_left_scale[:, None],
        product(rights, rows) * mixer_right_scale[:, None],
        channel_gain,
        spatial,
        spatial_bias,
    )
    total = scatter_sum(columns_out([[block[2] for block in mine] for mine in mixer], gated))
    stream = (stream.astype(jnp.float32) + total * scales[1][:, None]).astype(jnp.bfloat16)
    return half_step(
        stream, second_gain, second_rows, second_gate_scale, second_up_scale, second_cols, scales[2]
    )


def fits(stream, first_gate, mixer_left):
    groups, count, tps = lax.axis_size("grp"), lax.axis_size("fs"), lax.axis_size("tp")
    share = stream.shape[0] // groups
    tall = first_gate.shape[1] // 2
    return (
        groups == 2
        and count == 4
        and tps == 2 * CORES
        and first_gate.shape[0] == stream.shape[0]
        and share % LANES == 0
        and mixer_left.shape[1] == share
        and tall % 16 == 0
        and (2 * tall) % LANES == 0
        and stream.shape[1] % LANES == 0
    )


def fused(
    stream, first_gain, first_gate, first_gate_scale, first_up, first_up_scale, first_down, first_down_scale,
    mixer_gain, mixer_left, mixer_left_scale, mixer_right, mixer_right_scale, channel_gain, spatial,
    spatial_bias, mixer_out, mixer_out_scale, second_gain, second_gate, second_gate_scale, second_up,
    second_up_scale, second_down, second_down_scale,
):
    def flat(vector):
        return vector.reshape(1, -1)

    groups, count, tps = lax.axis_size("grp"), lax.axis_size("fs"), lax.axis_size("tp")
    wide, tokens = stream.shape
    share, tall, depth = wide // groups, first_gate.shape[1] // 2, wide * tps
    branch, part = mixer_left.shape[1], tokens // CHUNKS
    both = 2 * tokens
    any_spec, vmem = pl.BlockSpec(memory_space=pl.ANY), pl.BlockSpec(memory_space=pltpu.VMEM)
    chips = tps // CORES
    vm = pltpu.VMEM
    call = pl.pallas_call(
        kernel,
        out_shape=jax.ShapeDtypeStruct((wide, tokens), BF16),
        in_specs=[vmem] + [any_spec] * 9 + [vmem] * 15,
        out_specs=vmem,
        scratch_shapes=[
            vm((6, tall, depth), BF16),
            vm((count * groups, 3 * share, branch), BF16),
            vm((3, 2 * tall, share), BF16),
            vm((2 * tall, share), BF16),
            vm((2, share, 2 * tall), F32),
            vm((2 * tall, share), F32),
            vm((2, 3, share, branch), F32),
            vm((both, depth), BF16),
            vm((tokens, depth), BF16),
            vm((both, depth), BF16),
            vm((both, depth), BF16),
            vm((both, tall), BF16),
            vm((tokens, branch), BF16),
            vm((tokens, wide), BF16),
            vm((2 * CHUNKS, chips, part, wide), F32),
            vm((4, 8, tokens), F32),
            vm((2 * CHUNKS, chips, part, wide), BF16),
            vm((CHUNKS, chips, part, wide), BF16),
            vm((2 * CHUNKS, chips, part, wide), BF16),
            vm((CHUNKS, chips, part, wide), BF16),
            vm((2 * CHUNKS, chips, part, wide), BF16),
            vm((2 * CHUNKS, part, wide), BF16),
            vm((CHUNKS, part, wide), BF16),
            vm((2 * CHUNKS, part, wide), BF16),
            vm((CHUNKS, part, wide), BF16),
            vm((2 * CHUNKS, part, wide), BF16),
            vm((CHUNKS, part, wide), BF16),
            vm((CHUNKS, part, wide), BF16),
            vm((CHUNKS, part, wide), BF16),
            many(42 + 17 * CHUNKS + 12 * CHUNKS + 3),
            many(42 + 17 * CHUNKS + 12 * CHUNKS + 3),
            many(18),
        ],
        compiler_params=pltpu.CompilerParams(
            collective_id=0, has_side_effects=True, vmem_limit_bytes=67043328
        ),
    )
    return call(
        stream, first_gate, first_up, first_down, mixer_left, mixer_right, mixer_out,
        second_gate, second_up, second_down, flat(first_gain), flat(mixer_gain), flat(second_gain),
        flat(first_gate_scale), flat(first_up_scale), flat(first_down_scale), flat(mixer_left_scale),
        flat(mixer_right_scale), flat(mixer_out_scale), flat(second_gate_scale), flat(second_up_scale),
        flat(second_down_scale), flat(channel_gain), spatial, spatial_bias.T,
    )


def local(*args):
    if fits(args[0], args[2], args[9]):
        return fused(*args)
    return layer(*args)


def solution(mesh):
    return jax.shard_map(
        local,
        mesh=mesh,
        in_specs=(
            P("tp", ("grp", "fs")),
            P(),
            P("fs", "tp"),
            P("tp"),
            P("fs", "tp"),
            P("tp"),
            P("tp", "fs"),
            P("fs"),
            P(),
            P("fs", "tp"),
            P("tp"),
            P("fs", "tp"),
            P("tp"),
            P("tp"),
            P("tp", None, None),
            P("tp", None),
            P("tp", "fs"),
            P("fs"),
            P(),
            P("fs", "tp"),
            P("tp"),
            P("fs", "tp"),
            P("tp"),
            P("tp", "fs"),
            P("fs"),
        ),
        out_specs=P("tp", ("grp", "fs")),
        check_vma=False,
    )
```

profile of v0, /device:TPU:1, one launch (start us, length us, event | category | flops | bytes accessed | tf_op | source)
XLA Modules:
  0.0 287.0 jit_solution(11803317107561484710)
XLA Ops:
  0.0 1.3 reshape.42.gate_scale_1
  1.3 1.3 reshape.43.up_scale_1
  2.6 1.3 reshape.48.gate_scale_2
  3.9 1.3 reshape.49.up_scale_2
  5.2 1.4 copy.26
  6.6 278.6 %shard_map.235 = bf16[512,384]{1,0:T(8,128)(2,1)} custom-call(bf16[512,384]{1,0:T(8,128)(2,1)} %stream.1, f32[512,1408]{1,0:T(8,128)} %gate_1.1, f32[512,1408]{1,0:T(8,128)} %up_1.1, f32[1408,512]{1,0:T(8,128)} %down_1.1, f32[512,256]{1,0:T(8,128)} %left_w.1, f32[512,256]{1,0:T(8,128)} %right_w.1, f32[256,512]{1,0:T(8,128)} %out_w.1, f32[512,1408]{1,0:T(8,128)} %gate_2.1, ...), custom_call_target="tpu_custom_call" | custom-call | tf_op jit(solution)/shard_map/pallas_call | solution.py:864
  285.2 1.8 copy.28
where the time goes:
time: 288 us; the launch traced here: 287 us
  Pallas kernels  279 us (97%)
  local copies, waits for them, and re-layouts  8.36 us (3%)
    pallas_call x1, Pallas kernels, fused(): call(stream, first_gate, first_up, first_down, mixer_left, mixer_right, m...  279 us

commit v1 on v0

--- a/solution.py
+++ b/solution.py
@@ -8,7 +8,8 @@
 EPS = 1e-06
 CORES = 2
 LANES = 128
-CHUNKS = 2
+CHUNKS = 3
+PIECES = 2
 MESH = pl.DeviceIdType.MESH
 F32, BF16 = jnp.float32, jnp.bfloat16
 
@@ -72,6 +73,18 @@
         pending.append(copy)
         return copy
 
+    def reserve(source, target, device):
+        at = used[0]
+        used[0] += 1
+        return pltpu.make_async_remote_copy(
+            src_ref=source,
+            dst_ref=target,
+            send_sem=send_sem.at[at],
+            recv_sem=recv_sem.at[at],
+            device_id=device,
+            device_id_type=MESH,
+        )
+
     def sent(copies):
         for copy in copies:
             copy.wait_send()
@@ -110,7 +123,7 @@
     def turn(slot, scale, target):
         def step(at, carry):
             lanes = pl.ds(pl.multiple_of(at * LANES, LANES), LANES)
-            target[lanes, :] = (wide_in[slot, :, lanes] * scale[:, lanes]).T.astype(BF16)
+            target[lanes, :] = (wide_in[slot, :, lanes] * scale[lanes][None, :]).T.astype(BF16)
             return carry
 
         lax.fori_loop(0, wide_in.shape[2] // LANES, step, 0)
@@ -136,7 +149,7 @@
             mixer_in[slot, 2] * out_scale[:, of_share(member)]
         ).astype(BF16)
 
-    class Unit:
+    class Piece:
         def __init__(self, slot, source):
             self.slot, self.source = slot, source
 
@@ -148,8 +161,8 @@
         def relay_first(self):
             self.first.wait_recv()
             got = self.slot(partner, grp)
+            self.swaps = [send(got, got, to_group)]
             self.third = send(got, got, to_near)
-            self.swaps = [send(got, got, to_group)]
 
         def relay_second(self):
             self.second.wait_recv()
@@ -165,15 +178,50 @@
             for copy in self.swaps:
                 copy.wait_recv()
 
-    def hidden_unit(unit, stage, turns):
-        return Unit(
-            lambda source, member: weights.at[unit, :, place(source, member)],
-            lambda: staged.at[stage, other_side if turns else pl.ds(0, tall), :],
-        )
-
-    g1, u1, d1 = hidden_unit(0, 0, True), hidden_unit(1, 1, True), hidden_unit(2, 2, False)
-    g2, u2, d2 = hidden_unit(3, 0, True), hidden_unit(4, 1, True), hidden_unit(5, 2, False)
-    mixer = Unit(lambda source, member: mixer_w.at[source * groups + member], None)
+    def hidden_pieces(unit, stage, turns):
+        size = tall // PIECES
+
+        def piece(at):
+            first = at * size
+            away = (1 - side) * tall + first if turns else first
+            return Piece(
+                lambda source, member: weights.at[unit, pl.ds(first, size), place(source, member)],
+                lambda: staged.at[stage, pl.ds(pl.multiple_of(away, 16), size), :],
+            )
+
+        return [piece(at) for at in range(PIECES)]
+
+    def mixer_pieces():
+        size = mixer_w.shape[1] // PIECES
+
+        def piece(at):
+            rows = pl.ds(at * size, size)
+            return Piece(lambda source, member: mixer_w.at[source * groups + member, rows, :], None)
+
+        return [piece(at) for at in range(PIECES)]
+
+    pieces = (
+        hidden_pieces(0, 0, True) + hidden_pieces(1, 1, True) + hidden_pieces(2, 2, False) + mixer_pieces()
+        + hidden_pieces(3, 0, True) + hidden_pieces(4, 1, True) + hidden_pieces(5, 2, False)
+    )
+
+    begun_pieces = [2]
+
+    def ahead(at):
+        return 2 if at < 6 else 3
+
+    def pump(at):
+        pieces[at].relay_first()
+        pieces[at].relay_second()
+        for following in range(begun_pieces[0], min(at + ahead(at), len(pieces) - 1) + 1):
+            pieces[following].begin()
+            begun_pieces[0] += 1
+        if at > 0:
+            pieces[at - 1].relay_third()
+
+    def complete(first, last):
+        for piece in pieces[first * PIECES : last * PIECES]:
+            piece.complete()
 
 
     def gather_begin(rows, pair):
@@ -184,14 +232,18 @@
                 pl.ds(pl.multiple_of(at_tp * wide, wide), wide),
             ]
 
-        firsts, chips, cores = [], [], []
+        chips, cores = [], []
         for at in range(CHUNKS):
             mine = view(side, tp, at)
-            if pair:
-                firsts.append(send(mine, mine, to_partner))
             chips.append(send(mine, mine, to_across))
             cores.append(send(mine, mine, to_sibling))
-        return view, firsts, chips, cores
+        return view, [], chips, cores
+
+    def gather_pair(begun):
+        view, firsts, _, _ = begun
+        for at in range(CHUNKS):
+            mine = view(side, tp, at)
+            firsts.append(send(mine, mine, to_partner))
 
     def gather_end(begun):
         view, firsts, chips, cores = begun
@@ -300,6 +352,103 @@
 
         return product
 
+    class Targets:
+        def __init__(self, tiles, product):
+            self.tiles, self.product = tiles, product
+            self.order = (fs, partner, near, lax.rem(near + half, count))
+            every_tile = [(step, at) for step in range(len(self.order)) for at in range(len(tiles))]
+            self.cores = [
+                reserve(core_out.at[at, step % 2], core_in_2.at[at, step % 2], to_sibling)
+                for step, at in every_tile
+            ]
+            self.chips = [reserve(chip_out.at[at], chip_in_2.at[at], to_across) for _, at in every_tile]
+            self.pairs = [reserve(pair_out.at[at], pair_in_2.at[at], to_partner) for at in range(CHUNKS)]
+
+        def roles(self, step):
+            target = self.order[step]
+            hold = lax.rem(target, CORES) == core
+            here = target // CORES == chip
+            return target, hold, here
+
+        def begin(self, step):
+            target, hold, here = self.roles(step)
+            size = len(self.tiles)
+
+            def product(at):
+                value = self.product(self.tiles[at][0], target)
+
+                @pl.when(jnp.logical_not(hold))
+                def _():
+                    core_out[at, step % 2] = value.astype(BF16)
+                    self.cores[step * size + at].start()
+
+                @pl.when(hold)
+                def _():
+                    kept[at, here.astype(jnp.int32)] = value
+
+            def add(at):
+                @pl.when(hold)
+                def _():
+                    self.cores[step * size + at].wait_recv()
+                    slot = here.astype(jnp.int32)
+                    value = kept[at, slot] + core_in_2[at, step % 2].astype(F32)
+
+                    @pl.when(here)
+                    def _():
+                        kept[at, 1] = value
+
+                    @pl.when(jnp.logical_not(here))
+                    def _():
+                        chip_out[at] = value.astype(BF16)
+                        self.chips[step * size + at].start()
+
+            for at in range(size + 1):
+                if at < size:
+                    product(at)
+                if at > 0:
+                    add(at - 1)
+
+        def end(self, step):
+            _, hold, here = self.roles(step)
+            size = len(self.tiles)
+
+            @pl.when(jnp.logical_and(hold, here))
+            def _():
+                for at in range(size):
+                    self.chips[step * size + at].wait_recv()
+                    value = kept[at, 1] + chip_in_2[at].astype(F32)
+                    if self.tiles[at][1]:
+                        pair_out[at] = value.astype(BF16)
+                        self.pairs[at].start()
+                    else:
+                        kept[at, 1] = value
+
+        def finish(self):
+            own = [at for at in range(len(self.tiles)) if not self.tiles[at][1]]
+            for order, at in enumerate(own):
+                self.pairs[order].wait_recv()
+                total = kept[at, 1] + pair_in_2[order].astype(F32)
+                here = pl.ds(order * part, part)
+                held[here, :] = (held[here, :].astype(F32) + 0.5 * total).astype(BF16)
+
+        def drain(self):
+            size = len(self.tiles)
+            for step in range(len(self.order)):
+                _, hold, here = self.roles(step)
+
+                @pl.when(jnp.logical_not(hold))
+                def _(step=step):
+                    for at in range(size):
+                        self.cores[step * size + at].wait_send()
+
+                @pl.when(jnp.logical_and(hold, jnp.logical_not(here)))
+                def _(step=step):
+                    for at in range(size):
+                        self.chips[step * size + at].wait_send()
+
+            for copy in self.pairs:
+                copy.wait_send()
+
 
     def nothing(at):
         pass
@@ -307,64 +456,69 @@
     loads = {"g1": load_rows(gate_1, grp, 0), "u1": load_rows(up_1, grp, 1), "d1": load_cols(down_1, grp)}
     held[...] = stream[...].astype(F32).T.astype(BF16)
     own_rows(rows_1, True)
-    pl.semaphore_wait(barrier, len(every))
-    begun = gather_begin(rows_1, True)
-
     loads["g1"].wait()
     cast_rows(0, 0, 0, gate_scale_1)
-    g1.begin()
     loads["g1"] = load_rows(gate_1, 1 - grp, 0)
+    pl.semaphore_wait(barrier, len(every))
+    pieces[0].begin()
+    pieces[1].begin()
+    begun = gather_begin(rows_1, True)
     loads["u1"].wait()
     cast_rows(1, 1, 1, up_scale_1)
-    u1.begin()
     loads["u1"] = load_rows(up_1, 1 - grp, 1)
     loads["d1"].wait()
     cast_cols(2, 2, down_scale_1)
-    d1.begin()
     loads["d1"] = load_cols(down_1, 1 - grp)
     loads["m"] = load_mixer(grp, 0)
     loads["n"] = load_mixer(1 - grp, 1)
-    gather_end(begun)
-    g1.relay_first()
-    g1.relay_second()
     loads["g1"].wait()
     cast_rows(0, None, 0, gate_scale_1)
     loads["g2"] = load_rows(gate_2, grp, 0)
-    u1.relay_first()
-    u1.relay_second()
+    pump(0)
     loads["u1"].wait()
     cast_rows(1, None, 1, up_scale_1)
     loads["u2"] = load_rows(up_2, grp, 1)
-    d1.relay_first()
-    d1.relay_second()
+    pump(1)
     loads["d1"].wait()
     cast_cols(2, None, down_scale_1)
     loads["d2"] = load_cols(down_2, grp)
-    norm(rows_1, gain_1)
     for copy in loads["m"] + loads["n"]:
         copy.wait()
     cast_mixer(0, grp)
     cast_mixer(1, 1 - grp)
-    g1.relay_third()
-    sent([g1.first, u1.first, d1.first])
+    gather_pair(begun)
+    pump(2)
+    sent([piece.first for piece in pieces[0:2]])
     loads["g2"].wait()
     cast_rows(3, 0, 0, gate_scale_2)
     loads["g2"] = load_rows(gate_2, 1 - grp, 0)
-    u1.relay_third()
+    pump(3)
+    gather_end(begun)
+    pump(4)
+    norm(rows_1, gain_1)
+    sent([piece.first for piece in pieces[2:4]])
     loads["u2"].wait()
     cast_rows(4, 1, 1, up_scale_2)
     loads["u2"] = load_rows(up_2, 1 - grp, 1)
-    d1.relay_third()
-    mixer.begin()
-    g1.complete()
-    u1.complete()
+    pump(5)
+    sent([piece.first for piece in pieces[4:6]])
+    loads["d2"].wait()
+    cast_cols(5, 2, down_scale_2)
+    loads["d2"] = load_cols(down_2, 1 - grp)
+    loads["g2"].wait()
+    cast_rows(3, None, 0, gate_scale_2)
+    loads["u2"].wait()
+    cast_rows(4, None, 1, up_scale_2)
+    loads["d2"].wait()
+    cast_cols(5, None, down_scale_2)
+    pump(6)
+    complete(0, 2)
     expand(0)
-    d1.complete()
+    complete(2, 3)
 
     def between_1(at):
-        if at == 4:
-            mixer.relay_first()
-            mixer.relay_second()
+        if at == 3:
+            pump(7)
 
     copies = reduce_sums(
         half_tiles(), down_product(2), (core_out, chip_out, pair_out),
@@ -373,15 +527,10 @@
 
     own_rows(rows_m, False)
     begun = gather_begin(rows_m, False)
-    g2.begin()
-    u2.begin()
-    mixer.relay_third()
-    loads["d2"].wait()
-    cast_cols(5, 2, down_scale_2)
-    loads["d2"] = load_cols(down_2, 1 - grp)
+    pump(8)
     gather_end(begun)
     norm(rows_m, gain_m)
-    mixer.complete()
+    complete(3, 4)
 
     def projection(first):
         total = None
@@ -396,9 +545,9 @@
 
     right = projection(share)
     lane = lax.broadcasted_iota(jnp.int32, (tokens, LANES), 1)
-    sums = jnp.sum(right, axis=1, keepdims=True)
+    summed = jnp.sum(right, axis=1, keepdims=True)
     squares = jnp.sum(right * right, axis=1, keepdims=True)
-    packed = jnp.where(lane == 0, sums, jnp.where(lane == 1, squares, 0.0))
+    packed = jnp.where(lane == 0, summed, jnp.where(lane == 1, squares, 0.0))
     stats[0] = packed.T[0:8, :]
     shared = [
         send(stats.at[0], stats.at[1], to_sibling),
@@ -415,6 +564,8 @@
     inverse = lax.rsqrt(total[:, 1:2] / size - average * average + EPS)
     centred = ((right - average) * inverse * channel_gain[...]).astype(BF16)
     span = spatial.shape[1]
+    rest = jnp.zeros((span - spatial_bias.shape[0], span), F32)
+    bias = jnp.concatenate([spatial_bias[...], rest], axis=0).T
     target = lax.broadcasted_iota(jnp.int32, (span, span), 0)
     source = lax.broadcasted_iota(jnp.int32, (span, span), 1)
     members = branch // spatial.shape[0]
@@ -424,10 +575,9 @@
         for at in range(tokens // span):
             here = slice(at * span, (at + 1) * span)
             mixed = jnp.dot(matrix, centred[here, columns], preferred_element_type=F32)
-            mixed = mixed + spatial_bias[:, group : group + 1]
+            mixed = mixed + bias[:, group : group + 1]
             gated[here, columns] = (left[here, columns] * mixed).astype(BF16)
-    g2.relay_first()
-    g2.relay_second()
+    pump(9)
 
     def out_product(first, target):
         values = gated[first : first + part, :]
@@ -451,34 +601,40 @@
 
     own_rows(rows_2, True)
     begun = gather_begin(rows_2, True)
-    d2.begin()
-    u2.relay_first()
-    u2.relay_second()
-    g2.relay_third()
-    loads["g2"].wait()
-    cast_rows(3, None, 0, gate_scale_2)
-    loads["u2"].wait()
-    cast_rows(4, None, 1, up_scale_2)
-    loads["d2"].wait()
-    cast_cols(5, None, down_scale_2)
+    gather_pair(begun)
+    pump(10)
+    pump(11)
     gather_end(begun)
     norm(rows_2, gain_2)
-    u2.relay_third()
-    d2.relay_first()
-    d2.relay_second()
-    g2.complete()
-    u2.complete()
+    pump(12)
+    complete(4, 6)
     expand(3)
-    d2.relay_third()
-    d2.complete()
     sent(copies)
-    reduce_sums(
-        half_tiles(), down_product(5), (core_out, chip_out, pair_out),
-        (core_in_2, chip_in_2, pair_in_2), nothing,
-    )
+    sums = Targets(half_tiles(), down_product(5))
+    last = pieces[6 * PIECES :]
+
+    def arrived(step):
+        for piece in last:
+            piece.swaps[step].wait_recv()
+
+    sums.begin(0)
+    pump(13)
+    arrived(0)
+    sums.begin(1)
+    arrived(1)
+    sums.begin(2)
+    last[-1].relay_third()
+    sums.end(0)
+    sums.end(1)
+    arrived(2)
+    sums.begin(3)
+    sums.end(2)
+    sums.end(3)
+    sums.finish()
     result[...] = held[...].astype(F32).T.astype(BF16)
     for copy in list(pending):
         copy.wait_send()
+    sums.drain()
 
 
 def contract(left_side, right_side):
@@ -791,13 +947,15 @@
     return (
         groups == 2
         and count == 4
+        and count == tps
         and tps == 2 * CORES
         and first_gate.shape[0] == stream.shape[0]
         and share % LANES == 0
         and mixer_left.shape[1] == share
         and tall % 16 == 0
         and (2 * tall) % LANES == 0
-        and stream.shape[1] % LANES == 0
+        and stream.shape[1] % (LANES * CHUNKS) == 0
+        and tall % (16 * PIECES) == 0
     )
 
 
@@ -853,8 +1011,8 @@
             vm((CHUNKS, part, wide), BF16),
             vm((CHUNKS, part, wide), BF16),
             vm((CHUNKS, part, wide), BF16),
-            many(42 + 17 * CHUNKS + 12 * CHUNKS + 3),
-            many(42 + 17 * CHUNKS + 12 * CHUNKS + 3),
+            many(42 * PIECES + 73 * CHUNKS + 3),
+            many(42 * PIECES + 73 * CHUNKS + 3),
             many(18),
         ],
         compiler_params=pltpu.CompilerParams(
@@ -864,9 +1022,9 @@
     return call(
         stream, first_gate, first_up, first_down, mixer_left, mixer_right, mixer_out,
         second_gate, second_up, second_down, flat(first_gain), flat(mixer_gain), flat(second_gain),
-        flat(first_gate_scale), flat(first_up_scale), flat(first_down_scale), flat(mixer_left_scale),
-        flat(mixer_right_scale), flat(mixer_out_scale), flat(second_gate_scale), flat(second_up_scale),
-        flat(second_down_scale), flat(channel_gain), spatial, spatial_bias.T,
+        first_gate_scale, first_up_scale, flat(first_down_scale), flat(mixer_left_scale),
+        flat(mixer_right_scale), flat(mixer_out_scale), second_gate_scale, second_up_scale,
+        flat(second_down_scale), flat(channel_gain), spatial, spatial_bias,
     )
 
 

time: 288 us -> 259 us (0.90)
  Pallas kernels: 279 us -> 256 us
  local copies, waits for them, and re-layouts: 8.36 us -> 1.78 us
    pallas_call x1, Pallas kernels: 279 us -> 256 us  [fused(): call(stream, first_gate, first_up, first_down, mixer_left, mixer_right, m...]
    reshape x4 -> x0, local copies, waits for them, and re-layouts: 5.17 us -> none  [flat(): return vector.reshape(1, -1)]
where the time goes in v1:
time: 259 us; the launch traced here: 258 us
  Pallas kernels  256 us (99%)
    pallas_call x1, Pallas kernels, fused(): call(stream, first_gate, first_up, first_down, mixer_left, mixer_right, m...  256 us

profile of v1, /device:TPU:1, one launch (start us, length us, event | category | flops | bytes accessed | tf_op | source)
XLA Modules:
  0.0 258.1 jit_solution(16760864981581936630)
XLA Ops:
  0.0 256.3 %shard_map.235 = bf16[512,384]{1,0:T(8,128)(2,1)} custom-call(bf16[512,384]{1,0:T(8,128)(2,1)} %stream.1, f32[512,1408]{1,0:T(8,128)} %gate_1.1, f32[512,1408]{1,0:T(8,128)} %up_1.1, f32[1408,512]{1,0:T(8,128)} %down_1.1, f32[512,256]{1,0:T(8,128)} %left_w.1, f32[512,256]{1,0:T(8,128)} %right_w.1, f32[256,512]{1,0:T(8,128)} %out_w.1, f32[512,1408]{1,0:T(8,128)} %gate_2.1, ...), custom_call_target="tpu_custom_call" | custom-call | tf_op jit(solution)/shard_map/pallas_call | solution.py:1022
  256.3 1.8 copy.27

commit v2 on v1

--- a/solution.py
+++ b/solution.py
@@ -10,6 +10,9 @@
 LANES = 128
 CHUNKS = 3
 PIECES = 2
+SENDS = 40
+AHEAD = (2, 2, 2, 2, 1, 1, 2, 2, 3)
+SPLIT = 2
 MESH = pl.DeviceIdType.MESH
 F32, BF16 = jnp.float32, jnp.bfloat16
 
@@ -55,31 +58,36 @@
     for device in every:
         pl.semaphore_signal(barrier, inc=1, device_id=device, device_id_type=MESH)
 
-    used = [0, 0]
-    pending = []
+    used = [0, 0, SENDS]
+    pending, taken, slots = [], [], list(range(SENDS))
 
     def send(source, target, device):
+        if not slots:
+            sent([pending[0]])
+        slot = slots.pop(0)
         at = used[0]
         used[0] += 1
         copy = pltpu.make_async_remote_copy(
             src_ref=source,
             dst_ref=target,
-            send_sem=send_sem.at[at],
+            send_sem=send_sem.at[slot],
             recv_sem=recv_sem.at[at],
             device_id=device,
             device_id_type=MESH,
         )
         copy.start()
         pending.append(copy)
+        taken.append(slot)
         return copy
 
     def reserve(source, target, device):
         at = used[0]
         used[0] += 1
+        used[2] += 1
         return pltpu.make_async_remote_copy(
             src_ref=source,
             dst_ref=target,
-            send_sem=send_sem.at[at],
+            send_sem=send_sem.at[used[2] - 1],
             recv_sem=recv_sem.at[at],
             device_id=device,
             device_id_type=MESH,
@@ -87,8 +95,12 @@
 
     def sent(copies):
         for copy in copies:
-            copy.wait_send()
-        pending[:] = [other for other in pending if all(other is not copy for copy in copies)]
+            for at, other in enumerate(pending):
+                if other is copy:
+                    copy.wait_send()
+                    pending.pop(at)
+                    slots.append(taken.pop(at))
+                    break
 
     def load(source, target):
         at = used[1]
@@ -208,7 +220,7 @@
     begun_pieces = [2]
 
     def ahead(at):
-        return 2 if at < 6 else 3
+        return AHEAD[min(at, len(AHEAD) - 1)]
 
     def pump(at):
         pieces[at].relay_first()
@@ -216,8 +228,9 @@
         for following in range(begun_pieces[0], min(at + ahead(at), len(pieces) - 1) + 1):
             pieces[following].begin()
             begun_pieces[0] += 1
-        if at > 0:
-            pieces[at - 1].relay_third()
+
+    def third(at):
+        pieces[at].relay_third()
 
     def complete(first, last):
         for piece in pieces[first * PIECES : last * PIECES]:
@@ -241,22 +254,37 @@
 
     def gather_pair(begun):
         view, firsts, _, _ = begun
+        size = wide // SPLIT
         for at in range(CHUNKS):
             mine = view(side, tp, at)
-            firsts.append(send(mine, mine, to_partner))
-
-    def gather_end(begun):
-        view, firsts, chips, cores = begun
-        seconds = []
+            narrow = [mine.at[:, first * size : (first + 1) * size] for first in range(SPLIT)]
+            firsts.append([send(block, block, to_partner) for block in narrow])
+
+    def relay_own(begun):
+        view, _, chips, cores = begun
         for at in range(CHUNKS):
-            if firsts:
-                firsts[at].wait_recv()
-                got = view(1 - side, tp, at)
-                seconds.append(send(got, got, to_across))
-                cores.append(send(got, got, to_sibling))
             chips[at].wait_recv()
             got = view(side, across, at)
             cores.append(send(got, got, to_sibling))
+
+    def relay_pair(begun):
+        view, firsts, _, _ = begun
+        seconds, cores = [], []
+        for at in range(CHUNKS):
+            for copy in firsts[at]:
+                copy.wait_recv()
+            got = view(1 - side, tp, at)
+            seconds.append(send(got, got, to_across))
+            cores.append(send(got, got, to_sibling))
+        return seconds, cores
+
+    def end_own(begun):
+        for copy in begun[3]:
+            copy.wait_recv()
+
+    def end_pair(begun, relayed):
+        view = begun[0]
+        seconds, cores = relayed
         for at, copy in enumerate(seconds):
             copy.wait_recv()
             got = view(1 - side, across, at)
@@ -268,17 +296,17 @@
         first = pl.multiple_of(side * tokens, part) if pair else 0
         rows[pl.ds(first, tokens), pl.ds(pl.multiple_of(tp * wide, wide), wide)] = held[...]
 
-    def norm(rows, gain):
+    def norm(rows, gain, first):
         size = 64
 
         def step(at, carry):
-            here = pl.ds(pl.multiple_of(at * size, size), size)
+            here = pl.ds(pl.multiple_of(first + at * size, size), size)
             values = rows[here, :].astype(F32)
             inverse = lax.rsqrt(jnp.mean(values * values, axis=1, keepdims=True) + EPS)
             normal[here, :] = (values * inverse * gain[...]).astype(BF16)
             return carry
 
-        lax.fori_loop(0, rows.shape[0] // size, step, 0)
+        lax.fori_loop(0, tokens // size, step, 0)
 
     def expand(unit):
         def step(at, carry):
@@ -296,6 +324,8 @@
         core_to, chip_to, pair_to = outs
         core_from, chip_from, pair_from = ins
         firsts, seconds, thirds = {}, {}, {}
+        size = wide // SPLIT
+        halves = [slice(at * size, (at + 1) * size) for at in range(SPLIT)]
 
         def begin(at):
             for to_chip in range(tps // CORES):
@@ -317,7 +347,10 @@
             total = kept[at, chip] + chip_from[at].astype(F32)
             if tiles[at][1]:
                 pair_to[at] = total.astype(BF16)
-                thirds[at] = send(pair_to.at[at], pair_from.at[at], to_partner)
+                thirds[at] = [
+                    send(pair_to.at[at, :, columns], pair_from.at[at, :, columns], to_partner)
+                    for columns in halves
+                ]
             else:
                 kept[at, chip] = total
 
@@ -333,12 +366,13 @@
         for order, at in enumerate(own):
             total = kept[at, chip]
             if thirds:
-                thirds[order].wait_recv()
+                for copy in thirds[order]:
+                    copy.wait_recv()
                 total = total + pair_from[order].astype(F32)
             here = pl.ds(order * part, part)
             factor = 0.5 if thirds else 1.0
             held[here, :] = (held[here, :].astype(F32) + factor * total).astype(BF16)
-        return list(firsts.values()) + list(seconds.values()) + list(thirds.values())
+        return list(firsts.values()) + list(seconds.values()) + sum(thirds.values(), [])
 
     def half_tiles():
         away = [((1 - side) * tokens + at * part, True) for at in range(CHUNKS)]
@@ -356,12 +390,12 @@
         def __init__(self, tiles, product):
             self.tiles, self.product = tiles, product
             self.order = (fs, partner, near, lax.rem(near + half, count))
-            every_tile = [(step, at) for step in range(len(self.order)) for at in range(len(tiles))]
             self.cores = [
-                reserve(core_out.at[at, step % 2], core_in_2.at[at, step % 2], to_sibling)
-                for step, at in every_tile
+                reserve(core_out.at[at, step], core_in_2.at[at, step], to_sibling)
+                for step in range(2)
+                for at in range(len(tiles))
             ]
-            self.chips = [reserve(chip_out.at[at], chip_in_2.at[at], to_across) for _, at in every_tile]
+            self.chips = [reserve(chip_out.at[at], chip_in_2.at[at], to_across) for at in range(len(tiles))]
             self.pairs = [reserve(pair_out.at[at], pair_in_2.at[at], to_partner) for at in range(CHUNKS)]
 
         def roles(self, step):
@@ -370,9 +404,10 @@
             here = target // CORES == chip
             return target, hold, here
 
-        def begin(self, step):
+        def begin(self, step, pair):
             target, hold, here = self.roles(step)
             size = len(self.tiles)
+            chosen = [at for at in range(size) if self.tiles[at][1] == pair]
 
             def product(at):
                 value = self.product(self.tiles[at][0], target)
@@ -380,7 +415,7 @@
                 @pl.when(jnp.logical_not(hold))
                 def _():
                     core_out[at, step % 2] = value.astype(BF16)
-                    self.cores[step * size + at].start()
+                    self.cores[step % 2 * size + at].start()
 
                 @pl.when(hold)
                 def _():
@@ -389,7 +424,7 @@
             def add(at):
                 @pl.when(hold)
                 def _():
-                    self.cores[step * size + at].wait_recv()
+                    self.cores[step % 2 * size + at].wait_recv()
                     slot = here.astype(jnp.int32)
                     value = kept[at, slot] + core_in_2[at, step % 2].astype(F32)
 
@@ -400,22 +435,22 @@
                     @pl.when(jnp.logical_not(here))
                     def _():
                         chip_out[at] = value.astype(BF16)
-                        self.chips[step * size + at].start()
-
-            for at in range(size + 1):
-                if at < size:
-                    product(at)
-                if at > 0:
-                    add(at - 1)
-
-        def end(self, step):
+                        self.chips[at].start()
+
+            for order in range(len(chosen) + 1):
+                if order < len(chosen):
+                    product(chosen[order])
+                if order > 0:
+                    add(chosen[order - 1])
+
+        def end(self, step, pair):
             _, hold, here = self.roles(step)
-            size = len(self.tiles)
+            chosen = [at for at in range(len(self.tiles)) if self.tiles[at][1] == pair]
 
             @pl.when(jnp.logical_and(hold, here))
             def _():
-                for at in range(size):
-                    self.chips[step * size + at].wait_recv()
+                for at in chosen:
+                    self.chips[at].wait_recv()
                     value = kept[at, 1] + chip_in_2[at].astype(F32)
                     if self.tiles[at][1]:
                         pair_out[at] = value.astype(BF16)
@@ -439,19 +474,16 @@
                 @pl.when(jnp.logical_not(hold))
                 def _(step=step):
                     for at in range(size):
-                        self.cores[step * size + at].wait_send()
+                        self.cores[step % 2 * size + at].wait_send()
 
                 @pl.when(jnp.logical_and(hold, jnp.logical_not(here)))
                 def _(step=step):
                     for at in range(size):
-                        self.chips[step * size + at].wait_send()
+                        self.chips[at].wait_send()
 
             for copy in self.pairs:
                 copy.wait_send()
 
-
-    def nothing(at):
-        pass
 
     loads = {"g1": load_rows(gate_1, grp, 0), "u1": load_rows(up_1, grp, 1), "d1": load_cols(down_1, grp)}
     held[...] = stream[...].astype(F32).T.astype(BF16)
@@ -486,39 +518,55 @@
         copy.wait()
     cast_mixer(0, grp)
     cast_mixer(1, 1 - grp)
+    third(0)
     gather_pair(begun)
     pump(2)
     sent([piece.first for piece in pieces[0:2]])
     loads["g2"].wait()
     cast_rows(3, 0, 0, gate_scale_2)
     loads["g2"] = load_rows(gate_2, 1 - grp, 0)
+    third(1)
     pump(3)
-    gather_end(begun)
-    pump(4)
-    norm(rows_1, gain_1)
+    relay_own(begun)
+    relayed = relay_pair(begun)
+    third(2)
     sent([piece.first for piece in pieces[2:4]])
     loads["u2"].wait()
     cast_rows(4, 1, 1, up_scale_2)
     loads["u2"] = load_rows(up_2, 1 - grp, 1)
+    pump(4)
+    end_own(begun)
+    end_pair(begun, relayed)
+    norm(rows_1, gain_1, 0)
+    norm(rows_1, gain_1, tokens)
+    third(3)
+    loads["g2"].wait()
+    cast_rows(3, None, 0, gate_scale_2)
     pump(5)
     sent([piece.first for piece in pieces[4:6]])
     loads["d2"].wait()
     cast_cols(5, 2, down_scale_2)
     loads["d2"] = load_cols(down_2, 1 - grp)
-    loads["g2"].wait()
-    cast_rows(3, None, 0, gate_scale_2)
+    third(4)
     loads["u2"].wait()
     cast_rows(4, None, 1, up_scale_2)
     loads["d2"].wait()
     cast_cols(5, None, down_scale_2)
     pump(6)
+    third(5)
     complete(0, 2)
     expand(0)
     complete(2, 3)
 
     def between_1(at):
+        if at == 0:
+            pump(7)
         if at == 3:
-            pump(7)
+            third(6)
+        if at == 5:
+            pump(8)
+        if at == 7:
+            third(7)
 
     copies = reduce_sums(
         half_tiles(), down_product(2), (core_out, chip_out, pair_out),
@@ -527,9 +575,11 @@
 
     own_rows(rows_m, False)
     begun = gather_begin(rows_m, False)
-    pump(8)
-    gather_end(begun)
-    norm(rows_m, gain_m)
+    pump(9)
+    relay_own(begun)
+    end_own(begun)
+    norm(rows_m, gain_m, 0)
+    third(8)
     complete(3, 4)
 
     def projection(first):
@@ -555,6 +605,7 @@
         send(stats.at[0], stats.at[3], to_diagonal),
     ]
     left = projection(0)
+    pump(10)
     for copy in shared:
         copy.wait_recv()
     total = (stats[0] + stats[1]) + (stats[2] + stats[3])
@@ -577,7 +628,6 @@
             mixed = jnp.dot(matrix, centred[here, columns], preferred_element_type=F32)
             mixed = mixed + bias[:, group : group + 1]
             gated[here, columns] = (left[here, columns] * mixed).astype(BF16)
-    pump(9)
 
     def out_product(first, target):
         values = gated[first : first + part, :]
@@ -594,19 +644,31 @@
             axis=1,
         )
 
+    def between_m(at):
+        if at == 2:
+            third(9)
+        if at == 4:
+            pump(11)
+
     reduce_sums(
         [(at * part, False) for at in range(CHUNKS)], out_product, (core_out_m, chip_out_m, None),
-        (core_in_m, chip_in_m, None), nothing,
+        (core_in_m, chip_in_m, None), between_m,
     )
 
     own_rows(rows_2, True)
     begun = gather_begin(rows_2, True)
     gather_pair(begun)
-    pump(10)
-    pump(11)
-    gather_end(begun)
-    norm(rows_2, gain_2)
+    third(10)
+    relay_own(begun)
     pump(12)
+    third(11)
+    relayed = relay_pair(begun)
+    end_own(begun)
+    norm(rows_2, gain_2, side * tokens)
+    pump(13)
+    end_pair(begun, relayed)
+    norm(rows_2, gain_2, (1 - side) * tokens)
+    third(12)
     complete(4, 6)
     expand(3)
     sent(copies)
@@ -617,23 +679,27 @@
         for piece in last:
             piece.swaps[step].wait_recv()
 
-    sums.begin(0)
-    pump(13)
+    third(13)
+    sums.begin(0, True)
     arrived(0)
-    sums.begin(1)
+    sums.begin(1, True)
     arrived(1)
-    sums.begin(2)
-    last[-1].relay_third()
-    sums.end(0)
-    sums.end(1)
+    sums.begin(2, True)
+    sums.end(0, True)
+    sums.end(1, True)
     arrived(2)
-    sums.begin(3)
-    sums.end(2)
-    sums.end(3)
+    sums.begin(3, True)
+    sums.begin(0, False)
+    sums.begin(1, False)
+    sums.end(2, True)
+    sums.end(3, True)
+    sums.begin(2, False)
+    sums.begin(3, False)
+    for step in range(count):
+        sums.end(step, False)
     sums.finish()
     result[...] = held[...].astype(F32).T.astype(BF16)
-    for copy in list(pending):
-        copy.wait_send()
+    sent(list(pending))
     sums.drain()
 
 
@@ -954,6 +1020,7 @@
         and mixer_left.shape[1] == share
         and tall % 16 == 0
         and (2 * tall) % LANES == 0
+        and stream.shape[0] % (LANES * SPLIT) == 0
         and stream.shape[1] % (LANES * CHUNKS) == 0
         and tall % (16 * PIECES) == 0
     )
@@ -1011,8 +1078,8 @@
             vm((CHUNKS, part, wide), BF16),
             vm((CHUNKS, part, wide), BF16),
             vm((CHUNKS, part, wide), BF16),
-            many(42 * PIECES + 73 * CHUNKS + 3),
-            many(42 * PIECES + 73 * CHUNKS + 3),
+            many(SENDS + 7 * CHUNKS),
+            many(42 * PIECES + (28 + 3 * SPLIT) * CHUNKS + 3),
             many(18),
         ],
         compiler_params=pltpu.CompilerParams(

time: 259 us -> 236 us (0.911)
  Pallas kernels: 256 us -> 234 us
    pallas_call x1, Pallas kernels: 256 us -> 234 us  [fused(): call(stream, first_gate, first_up, first_down, mixer_left, mixer_right, m...]
where the time goes in v2:
time: 236 us
  Pallas kernels  234 us (99%)
    pallas_call x1, Pallas kernels, fused(): call(stream, first_gate, first_up, first_down, mixer_left, mixer_right, m...  234 us

profile of v2, /device:TPU:1, one launch (start us, length us, event | category | flops | bytes accessed | tf_op | source)
XLA Modules:
  0.0 235.9 jit_solution(14458567145081465166)
XLA Ops:
  0.0 234.2 %shard_map.235 = bf16[512,384]{1,0:T(8,128)(2,1)} custom-call(bf16[512,384]{1,0:T(8,128)(2,1)} %stream.1, f32[512,1408]{1,0:T(8,128)} %gate_1.1, f32[512,1408]{1,0:T(8,128)} %up_1.1, f32[1408,512]{1,0:T(8,128)} %down_1.1, f32[512,256]{1,0:T(8,128)} %left_w.1, f32[512,256]{1,0:T(8,128)} %right_w.1, f32[256,512]{1,0:T(8,128)} %out_w.1, f32[512,1408]{1,0:T(8,128)} %gate_2.1, ...), custom_call_target="tpu_custom_call" | custom-call | tf_op jit(solution)/shard_map/pallas_call | solution.py:1089
  234.2 1.8 copy.27
